TPU v7x, 512 devices: a 4x2x32 block of a 4x8x32 slice. The times are simulated.
512 devices in a mesh: grp: 2 (over y), fs: 32 (over z), tp: 8 (over x, core).
Axes of the slice: x: 4, y: 2, z: 32, core: 2. Of those that a mesh axis runs over, the one named last changes fastest.
The devices are a block of a 4x8x32 slice.
Arguments:
- tokens: bfloat16 [16384, 2048], P(('grp', 'fs'), 'tp'), parts along dimension 0, may hold values from -6 to 6
- recurrent_norm_gain: float32 [2048], replicated, may hold values from 0.1 to 1.9
- feedforward_norm_gain: float32 [2048], replicated, may hold values from 0.1 to 1.9
- gate_projection_weight: bfloat16 [2048, 2048], P('fs', 'tp'), may hold values from -0.125 to 0.125
- recurrent_projection_weight: bfloat16 [2048, 2048], P('fs', 'tp'), may hold values from -0.125 to 0.125
- convolution_kernel: bfloat16 [4, 2048], P(None, 'tp'), may hold values from -3 to 3
- decay_gate_matrix: bfloat16 [16, 128, 128], P('tp'), may hold values from -0.5 to 0.5
- input_gate_matrix: bfloat16 [16, 128, 128], P('tp'), may hold values from -0.5 to 0.5
- base_decay_logit: float32 [2048], P('tp'), may hold values from 3 to 9
- extra_log_decay: float32 [16384], P(('grp', 'fs')), parts along dimension 0, may hold values from -0.7 to 0
- output_projection_weight: bfloat16 [2048, 2048], P('tp', 'fs'), may hold values from -0.125 to 0.125
- up_projection_weight: bfloat16 [2048, 8192], P('fs', 'tp'), may hold values from -0.125 to 0.125
- down_projection_weight: bfloat16 [8192, 2048], P('tp', 'fs'), may hold values from -0.0625 to 0.0625
Outputs:
- layer_out: bfloat16 [16384, 2048], P(('grp', 'fs'), 'tp'), parts along dimension 0
There are 2 independent parts, one for each index of `grp`. A program takes and returns all parts, laid end to end along the dimension named above; an argument that names none is the same for every part. Nothing has to cross between parts.
All inputs are finite; a program needn't handle non-finite values.
Results may differ from a plain program's by a relative error of at most 0.018.
Values may be sent and summed in bfloat16 or wider, within the bound.
No kernel may reach another device: no remote copies, remote signals or barrier semaphores. Data moves between devices by JAX's collectives and lax.ppermute only.
A program may use at most 64 MiB of HBM per device.

v0:
```python
import jax
import jax.numpy as jnp
from jax import lax
from jax.sharding import PartitionSpec as P


def from_everyone(x, axis):
    copies = jnp.broadcast_to(x, (lax.axis_size(axis), *x.shape))
    return lax.all_to_all(copies, axis, split_axis=0, concat_axis=0, tiled=True)


def laid_out(tiles, dim):
    tiles = jnp.moveaxis(tiles, 0, dim)
    lengths = tiles.shape
    return tiles.reshape(*lengths[:dim], lengths[dim] * lengths[dim + 1], *lengths[dim + 2 :])


def collect(x, axis, dim):
    tiles = from_everyone(x, axis)
    return laid_out(tiles, dim)


def gather_turned(arrays, axis, dims):
    turned = [jnp.moveaxis(a, dim, 0) for a, dim in zip(arrays, dims)]
    widths = [t[0].size for t in turned]
    both = jnp.concatenate([t.reshape(-1, w) for t, w in zip(turned, widths)], axis=1)
    out = lax.all_gather(both, axis, axis=0, tiled=True)
    tiles = jnp.split(out, [sum(widths[:k]) for k in range(1, len(widths))], axis=1)
    return tuple(
        (
            jnp.moveaxis(b.reshape(-1, *t.shape[1:]), 0, dim)
            for b, t, dim in zip(tiles, turned, dims)
        )
    )


def in_blocks(x, dim, peers):
    lengths = x.shape
    tiles = x.reshape(*lengths[:dim], peers, lengths[dim] // peers, *lengths[dim + 1 :])
    return jnp.moveaxis(tiles, dim, 0)


def sent_and_summed(x, axis, dim):
    peers = lax.axis_size(axis)
    tiles = lax.all_to_all(in_blocks(x, dim, peers), axis, 0, 0, tiled=True)
    return jnp.sum(tiles.astype(jnp.float32), axis=0)


def rms_rows(values_in, norm_gain):
    values = values_in.astype(jnp.float32)
    inverse = lax.rsqrt(jnp.mean(values * values, axis=-1, keepdims=True) + 1e-06)
    return (values * inverse * norm_gain).astype(jnp.bfloat16)


def combine(earlier, later):
    return (earlier[0] * later[0], later[0] * earlier[1] + later[1])


def recurrent_state(
    recurrent_branch_rows,
    gate_branch_rows,
    convolution_kernel,
    decay_gate_matrix,
    input_gate_matrix,
    base_decay_logit,
    extra_log_decay,
):
    length = recurrent_branch_rows.shape[0]
    taps = convolution_kernel.shape[0]
    padded = jnp.pad(recurrent_branch_rows.astype(jnp.float32), ((taps - 1, 0), (0, 0)))
    conv_sum = jnp.zeros((length, recurrent_branch_rows.shape[1]), jnp.float32)
    for tap_index in range(taps):
        conv_sum = conv_sum + padded[tap_index : tap_index + length] * convolution_kernel[
            tap_index
        ].astype(jnp.float32)
    conv_rows = conv_sum.astype(jnp.bfloat16)
    blocks = decay_gate_matrix.shape[0]
    blocked = conv_rows.reshape(length, blocks, -1)
    recurrence_gate = jax.nn.sigmoid(
        jnp.einsum(
            "tni,nij->tnj", blocked, decay_gate_matrix, preferred_element_type=jnp.float32
        ).reshape(length, -1)
    )
    input_rate = jax.nn.sigmoid(
        jnp.einsum(
            "tni,nij->tnj", blocked, input_gate_matrix, preferred_element_type=jnp.float32
        ).reshape(length, -1)
    )
    decay_log_values = (
        -8.0 * jax.nn.softplus(-base_decay_logit) * recurrence_gate + extra_log_decay[:, None]
    )
    decay = jnp.exp(decay_log_values)
    drive = (
        jnp.sqrt(-jnp.expm1(2.0 * decay_log_values)) * input_rate * conv_rows.astype(jnp.float32)
    )
    _, hidden = lax.associative_scan(combine, (decay, drive), axis=0)
    return (hidden * gate_branch_rows.astype(jnp.float32)).astype(jnp.bfloat16)


def per_device(
    tokens,
    recurrent_norm_gain,
    feedforward_norm_gain,
    gate_projection_weight,
    recurrent_projection_weight,
    convolution_kernel,
    decay_gate_matrix,
    input_gate_matrix,
    base_decay_logit,
    extra_log_decay,
    output_projection_weight,
    up_projection_weight,
    down_projection_weight,
):
    whole_rows = collect(tokens, "tp", 1)
    normed = rms_rows(whole_rows, recurrent_norm_gain)
    gate_whole, recur_whole, out_whole, up_whole, down_whole = gather_turned(
        (
            gate_projection_weight,
            recurrent_projection_weight,
            output_projection_weight,
            up_projection_weight,
            down_projection_weight,
        ),
        "fs",
        (0, 0, 1, 0, 1),
    )
    gate_pre = jnp.dot(normed, gate_whole, preferred_element_type=jnp.float32)
    recur_pre = jnp.dot(normed, recur_whole, preferred_element_type=jnp.float32)
    gate_branch_rows = jax.nn.gelu(gate_pre).astype(jnp.bfloat16)
    recurrent_branch_rows = recur_pre.astype(jnp.bfloat16)
    mixed_output = recurrent_state(
        recurrent_branch_rows,
        gate_branch_rows,
        convolution_kernel,
        decay_gate_matrix,
        input_gate_matrix,
        base_decay_logit,
        extra_log_decay,
    )
    partials = jnp.dot(mixed_output, out_whole, preferred_element_type=jnp.float32)
    residual = (
        tokens.astype(jnp.float32) + sent_and_summed(partials.astype(jnp.bfloat16), "tp", 1)
    ).astype(jnp.bfloat16)
    middle = collect(residual, "tp", 1)
    channel_in = rms_rows(middle, feedforward_norm_gain)
    upward = jnp.dot(channel_in, up_whole, preferred_element_type=jnp.float32)
    positive = jnp.maximum(upward, 0.0)
    squared = (positive * positive).astype(jnp.bfloat16)
    down_terms = jnp.dot(squared, down_whole, preferred_element_type=jnp.float32)
    summed_down = sent_and_summed(down_terms.astype(jnp.bfloat16), "tp", 1)
    return (residual.astype(jnp.float32) + summed_down).astype(jnp.bfloat16)


def solution(mesh):
    placed = (
        P(("grp", "fs"), "tp"),
        P(),
        P(),
        P("fs", "tp"),
        P("fs", "tp"),
        P(None, "tp"),
        P("tp", None, None),
        P("tp", None, None),
        P("tp"),
        P(("grp", "fs")),
        P("tp", "fs"),
        P("fs", "tp"),
        P("tp", "fs"),
    )
    return jax.shard_map(
        per_device, mesh=mesh, in_specs=placed, out_specs=P(("grp", "fs"), "tp"), check_vma=False
    )
```

profile of v0, /device:TPU:33, one launch (start us, length us, event | category | flops | bytes accessed | tf_op | source)
XLA Modules:
  0.0 277.3 jit_solution(16878927813386436569)
XLA Ops:
  6.6 0.8 constant_dynamic-update-slice_fusion.2
  7.3 0.8 constant_dynamic-update-slice_fusion.1
  8.1 0.8 bitcast_dynamic-update-slice_fusion.1
  8.9 0.9 constant_dynamic-update-slice_fusion
  9.8 0.9 bitcast_dynamic-update-slice_fusion
  10.7 0.7 copy-done.2
  11.6 1.0 copy.28
  12.6 1.1 broadcast_in_dim.4
  13.6 44.9 %all-to-all-start = ((bf16[8,256,256]{1,2,0:T(8,128)(2,1)}), bf16[8,256,256]{1,2,0:T(8,128)(2,1)S(1)}, u32[]{:S(2)}, u32[]{:S(2)}) async-start(bf16[8,256,256]{1,2,0:T(8,128)(2,1)} %broadcast_in_dim.4), calls=%async_computation | async-start | bytes 2097152 | tf_op jit(solution)/shard_map/all_to_all | solution.py:9
  58.6 15.0 %all-to-all-done = bf16[8,256,256]{1,2,0:T(8,128)(2,1)S(1)} async-done(((bf16[8,256,256]{1,2,0:T(8,128)(2,1)}), bf16[8,256,256]{1,2,0:T(8,128)(2,1)S(1)}, u32[]{:S(2)}, u32[]{:S(2)}) %all-to-all-start) | async-done | bytes 1048608 | tf_op jit(solution)/shard_map/all_to_all | solution.py:9
  73.6 0.3 multiply_reduce_fusion.1
  73.9 0.3 fusion.10
  74.3 112.4 %all-gather.2.cloned.1.call-done = bf16[2048,2816]{1,0:T(8,128)(2,1)} async-done(((bf16[64,2816]{1,0:T(8,128)(2,1)}), bf16[2048,2816]{1,0:T(8,128)(2,1)}) %all-gather.2.cloned.1.call-update) | async-done | bytes 11534352 | tf_op jit(solution)/shard_map/all_gather | solution.py:27
  186.7 1.7 fusion.28
  188.6 0.3 fusion.24
  189.4 0.3 fusion.59
  192.3 2.9 %convolution_convert_fusion = bf16[256,2048]{1,0:T(8,128)(2,1)S(1)} fusion(bf16[2048,2816]{1,0:T(8,128)(2,1)} %all-gather.2.cloned.1.call-done, bf16[256,2048]{0,1:T(8,128)(2,1)S(1)} %fusion.10, f32[256,256]{1,0:T(8,128)S(1)} %pad.68, f32[256,256]{1,0:T(8,128)S(1)} %pad.69), kind=kOutput, calls=%fused_computation.5 | convolution fusion | flops 538247168 | bytes 4718592 | tf_op jit(solution)/shard_map/dot_general | solution.py:141
  195.3 30.4 %all_to_all.20 = bf16[8,256,256]{2,1,0:T(8,128)(2,1)S(1)} all-to-all(bf16[8,256,256]{2,1,0:T(8,128)(2,1)S(1)} %bitcast.56), channel_id=1, replica_groups=mesh['grp'=2,'fs'=32,'tp'=8] {'tp'}, dimensions={0} | all-to-all | bytes 2097152 | tf_op jit(solution)/shard_map/all_to_all | solution.py:45
  226.0 18.5 %all_to_all.21 = bf16[8,256,256]{1,2,0:T(8,128)(2,1)S(1)} all-to-all(bf16[8,256,256]{1,2,0:T(8,128)(2,1)S(1)} %broadcast_in_dim.5), channel_id=1, replica_groups=mesh['grp'=2,'fs'=32,'tp'=8] {'tp'}, dimensions={0} | all-to-all | bytes 2097152 | tf_op jit(solution)/shard_map/all_to_all | solution.py:9
  244.5 0.3 multiply_reduce_fusion
  244.8 0.3 fusion.8
  245.2 5.8 %fusion.4 = bf16[256,2048]{1,0:T(8,128)(2,1)S(1)} fusion(bf16[2048,2816]{1,0:T(8,128)(2,1)} %all-gather.2.cloned.1.call-done, bf16[256,2048]{0,1:T(8,128)(2,1)S(1)} %fusion.8), kind=kOutput, calls=%fused_computation.4 | convolution fusion | flops 2148794368 | bytes 10485760 | tf_op jit(solution)/shard_map/dot_general | solution.py:150
  251.1 18.5 %all_to_all.22 = bf16[8,256,256]{2,1,0:T(8,128)(2,1)S(1)} all-to-all(bf16[8,256,256]{2,1,0:T(8,128)(2,1)S(1)} %bitcast.57), channel_id=1, replica_groups=mesh['grp'=2,'fs'=32,'tp'=8] {'tp'}, dimensions={0} | all-to-all | bytes 2097152 | tf_op jit(solution)/shard_map/all_to_all | solution.py:45
  269.7 0.7 add_convert_fusion
  (123 shorter events, 3.5 us)
Async XLA Ops:
  6.5 182.0 %copy-start = (bf16[2,128,128]{2,1,0:T(8,128)(2,1)S(1)}, bf16[2,128,128]{2,1,0:T(8,128)(2,1)}, u32[]{:S(2)}) copy-start(bf16[2,128,128]{2,1,0:T(8,128)(2,1)} %param.20) | copy-start | bytes 196612
  6.6 180.2 %all-gather.2.cloned.1.call-start = ((), (), s32[]{:S(2)}) async-start(), calls=%async_computation.4 | async-start | bytes 11894784 | tf_op jit(solution)/shard_map/all_gather | solution.py:27
  9.8 48.8 %copy-start.7 = (f32[256]{0:T(256)S(1)}, f32[256]{0:T(256)}, u32[]{:S(2)}) copy-start(f32[256]{0:T(256)} %param.21) | copy-start | bytes 3076
  9.8 48.8 %copy-start.5 = (bf16[4,256]{1,0:T(4,128)(2,1)S(1)}, bf16[4,256]{1,0:T(4,128)(2,1)}, u32[]{:S(2)}) copy-start(bf16[4,256]{1,0:T(4,128)(2,1)} %param.18) | copy-start | bytes 6148
  10.7 0.8 copy-start.2
  12.6 61.4 %copy-start.3 = (f32[2048]{0:T(1024)S(1)}, f32[2048]{0:T(1024)}, u32[]{:S(2)}) copy-start(f32[2048]{0:T(1024)} %param.14) | copy-start | bytes 24580
  13.6 60.0 %all-to-all-start = ((bf16[8,256,256]{1,2,0:T(8,128)(2,1)}), bf16[8,256,256]{1,2,0:T(8,128)(2,1)S(1)}, u32[]{:S(2)}, u32[]{:S(2)}) async-start(bf16[8,256,256]{1,2,0:T(8,128)(2,1)} %broadcast_in_dim.4), calls=%async_computation | async-start | bytes 2097152 | tf_op jit(solution)/shard_map/all_to_all | solution.py:9
  74.3 114.7 %copy-start.8 = (bf16[2,128,128]{2,1,0:T(8,128)(2,1)S(1)}, bf16[2,128,128]{2,1,0:T(8,128)(2,1)}, u32[]{:S(2)}) copy-start(bf16[2,128,128]{2,1,0:T(8,128)(2,1)} %param.19) | copy-start | bytes 196612
  188.4 1.0 copy-start.6
  195.3 30.5 %copy-start.1 = (bf16[256,256]{1,0:T(8,128)(2,1)S(1)}, bf16[256,256]{1,0:T(8,128)(2,1)}, u32[]{:S(2)}) copy-start(bf16[256,256]{1,0:T(8,128)(2,1)} %param.13) | copy-start | bytes 393220
  226.0 18.9 %copy-start.4 = (f32[2048]{0:T(1024)S(1)}, f32[2048]{0:T(1024)}, u32[]{:S(2)}) copy-start(f32[2048]{0:T(1024)} %param.15) | copy-start | bytes 24580
Sparse Core Ops, SparseCore 0:
  11.7 174.9 all-gather.1
where the time goes:
time: 278 us; the launch traced here: 277 us
  waiting for transfers between devices  128 us (46%)
  blocking collectives  67.3 us (24%)
  starting transfers between devices  44.9 us (16%)
  between operations  14.1 us (5%)
  matrix products  11 us (4%)
  local copies, waits for them, and re-layouts  9.37 us (3%)
  other arithmetic  3.14 us (1%)
    all_gather x1, waiting for transfers between devices, gather_turned(): out = lax.all_gather(both, axis, axis=0, tiled=True)  112 us
    all_to_all x2, blocking collectives, sent_and_summed(): tiles = lax.all_to_all(in_blocks(x, dim, peers), axis, 0, 0, tiled=True)  48.8 us
    all_to_all x1, starting transfers between devices, from_everyone(): return lax.all_to_all(copies, axis, split_axis=0, concat_axis=0, tiled=True)  44.9 us
    all_to_all x1, blocking collectives, from_everyone(): return lax.all_to_all(copies, axis, split_axis=0, concat_axis=0, tiled=True)  18.5 us
    all_to_all x1, waiting for transfers between devices, from_everyone(): return lax.all_to_all(copies, axis, split_axis=0, concat_axis=0, tiled=True)  15 us
    dot_general x1, matrix products, per_device(): jnp.dot(squared, down_whole, preferred_element_type=jnp.float32)  5.84 us
  transfers between devices with their start and end apart: 2, of which 2 were waited for; matrix products, arithmetic and copies ran while one was open for 1% of the time, Pallas kernels for 0%

commit v1 on v0

--- a/solution.py
+++ b/solution.py
@@ -2,6 +2,13 @@
 import jax.numpy as jnp
 from jax import lax
 from jax.sharding import PartitionSpec as P
+
+
+def gather_over(shard, axis, along):
+    devices = lax.axis_size(axis)
+    parts = jnp.stack([shard for _ in range(devices)])
+    parts = lax.all_to_all(parts, axis, split_axis=0, concat_axis=0)
+    return jnp.concatenate(parts, axis=along)
 
 
 def from_everyone(x, axis):
@@ -24,7 +31,7 @@
     turned = [jnp.moveaxis(a, dim, 0) for a, dim in zip(arrays, dims)]
     widths = [t[0].size for t in turned]
     both = jnp.concatenate([t.reshape(-1, w) for t, w in zip(turned, widths)], axis=1)
-    out = lax.all_gather(both, axis, axis=0, tiled=True)
+    out = gather_over(both, axis, 0)
     tiles = jnp.split(out, [sum(widths[:k]) for k in range(1, len(widths))], axis=1)
     return tuple(
         (

time: 278 us -> 1150 us (4.14)
  the two profiles are of different devices: /device:TPU:33 before, /device:TPU:232 now
where the time goes in v1:
time: 1150 us
  waiting for transfers between devices  1020 us (89%)
  blocking collectives  55.6 us (5%)
  starting transfers between devices  46.4 us (4%)
    all_to_all x1, waiting for transfers between devices, gather_over(): parts = lax.all_to_all(parts, axis, split_axis=0, concat_axis=0)  1010 us
    all_to_all x1, starting transfers between devices, gather_over(): parts = lax.all_to_all(parts, axis, split_axis=0, concat_axis=0)  41.8 us
    all_to_all x2, blocking collectives, sent_and_summed(): tiles = lax.all_to_all(in_blocks(x, dim, peers), axis, 0, 0, tiled=True)  37.1 us
  transfers between devices with their start and end apart: 2, of which 2 were waited for; matrix products, arithmetic and copies ran while one was open for 0% of the time, Pallas kernels for 0%

profile of v1, /device:TPU:232, one launch (start us, length us, event | category | flops | bytes accessed | tf_op | source)
XLA Modules:
  0.0 1147.9 jit_solution(8582600106492224976)
XLA Ops:
  0.0 1.1 copy.28
  1.1 1.0 broadcast_in_dim.4
  2.2 4.6 all-to-all-start
  6.9 15.8 %all-to-all-done = bf16[8,256,256]{1,2,0:T(8,128)(2,1)S(1)} async-done(((bf16[8,256,256]{1,2,0:T(8,128)(2,1)}), bf16[8,256,256]{1,2,0:T(8,128)(2,1)S(1)}, u32[]{:S(2)}, u32[]{:S(2)}) %all-to-all-start) | async-done | bytes 1048608 | tf_op jit(solution)/shard_map/all_to_all | solution.py:16
  22.7 5.5 stack.2
  28.2 41.8 %all-to-all-start.1 = ((bf16[32,64,2816]{2,1,0:T(8,128)(2,1)}), bf16[32,64,2816]{2,1,0:T(8,128)(2,1)}, u32[]{:S(2)}, u32[]{:S(2)}) async-start(bf16[32,64,2816]{2,1,0:T(8,128)(2,1)} %stack.2), calls=%async_computation.1 | async-start | bytes 23068672 | tf_op jit(solution)/shard_map/all_to_all | solution.py:10
  70.1 0.3 multiply_reduce_fusion.1
  70.4 0.3 fusion.10
  70.8 1005.2 %all-to-all-done.1 = bf16[32,64,2816]{2,1,0:T(8,128)(2,1)} async-done(((bf16[32,64,2816]{2,1,0:T(8,128)(2,1)}), bf16[32,64,2816]{2,1,0:T(8,128)(2,1)}, u32[]{:S(2)}, u32[]{:S(2)}) %all-to-all-start.1) | async-done | bytes 11534368 | tf_op jit(solution)/shard_map/all_to_all | solution.py:10
  1075.9 1.7 fusion.28
  1077.8 0.3 fusion.27
  1078.2 0.3 fusion.24
  1078.7 0.3 fusion.59
  1079.0 0.2 slice.213
  1079.5 0.2 slice.270
  1081.6 2.9 convolution_convert_fusion
  1084.6 18.6 %all_to_all.25 = bf16[8,256,256]{2,1,0:T(8,128)(2,1)S(1)} all-to-all(bf16[8,256,256]{2,1,0:T(8,128)(2,1)S(1)} %bitcast.57), channel_id=1, replica_groups=mesh['grp'=2,'fs'=32,'tp'=8] {'tp'}, dimensions={0} | all-to-all | bytes 2097152 | tf_op jit(solution)/shard_map/all_to_all | solution.py:52
  1103.6 18.5 %all_to_all.26 = bf16[8,256,256]{1,2,0:T(8,128)(2,1)S(1)} all-to-all(bf16[8,256,256]{1,2,0:T(8,128)(2,1)S(1)} %broadcast_in_dim.5), channel_id=1, replica_groups=mesh['grp'=2,'fs'=32,'tp'=8] {'tp'}, dimensions={0} | all-to-all | bytes 2097152 | tf_op jit(solution)/shard_map/all_to_all | solution.py:16
  1122.0 0.3 multiply_reduce_fusion
  1122.3 0.3 fusion.8
  1122.7 5.8 fusion.4
  1128.6 18.5 %all_to_all.27 = bf16[8,256,256]{2,1,0:T(8,128)(2,1)S(1)} all-to-all(bf16[8,256,256]{2,1,0:T(8,128)(2,1)S(1)} %bitcast.58), channel_id=1, replica_groups=mesh['grp'=2,'fs'=32,'tp'=8] {'tp'}, dimensions={0} | all-to-all | bytes 2097152 | tf_op jit(solution)/shard_map/all_to_all | solution.py:52
  1147.1 0.1 convert_reduce_fusion
  1147.2 0.7 add_convert_fusion
  (131 shorter events, 2.7 us)
Async XLA Ops:
  0.0 1077.8 %copy-start = (bf16[2,128,128]{2,1,0:T(8,128)(2,1)S(1)}, bf16[2,128,128]{2,1,0:T(8,128)(2,1)}, u32[]{:S(2)}) copy-start(bf16[2,128,128]{2,1,0:T(8,128)(2,1)} %param.19) | copy-start | bytes 196612
  0.0 6.7 copy-start.4
  0.0 6.8 copy-start.5
  0.0 6.8 copy-start.6
  0.0 6.8 copy-start.2
  0.0 6.8 copy-start.3
  2.2 20.5 %all-to-all-start = ((bf16[8,256,256]{1,2,0:T(8,128)(2,1)}), bf16[8,256,256]{1,2,0:T(8,128)(2,1)S(1)}, u32[]{:S(2)}, u32[]{:S(2)}) async-start(bf16[8,256,256]{1,2,0:T(8,128)(2,1)} %broadcast_in_dim.4), calls=%async_computation | async-start | bytes 2097152 | tf_op jit(solution)/shard_map/all_to_all | solution.py:16
  28.2 41.8 %copy-start.11 = (f32[256]{0:T(256)S(1)}, f32[256]{0:T(256)}, u32[]{:S(2)}) copy-start(f32[256]{0:T(256)} %param.21) | copy-start | bytes 3076
  28.2 41.9 %copy-start.9 = (bf16[4,256]{1,0:T(4,128)(2,1)S(1)}, bf16[4,256]{1,0:T(4,128)(2,1)}, u32[]{:S(2)}) copy-start(bf16[4,256]{1,0:T(4,128)(2,1)} %param.18) | copy-start | bytes 6148
  28.2 42.2 %copy-start.7 = (f32[2048]{0:T(1024)S(1)}, f32[2048]{0:T(1024)}, u32[]{:S(2)}) copy-start(f32[2048]{0:T(1024)} %param.14) | copy-start | bytes 24580
  28.2 1047.7 %all-to-all-start.1 = ((bf16[32,64,2816]{2,1,0:T(8,128)(2,1)}), bf16[32,64,2816]{2,1,0:T(8,128)(2,1)}, u32[]{:S(2)}, u32[]{:S(2)}) async-start(bf16[32,64,2816]{2,1,0:T(8,128)(2,1)} %stack.2), calls=%async_computation.1 | async-start | bytes 23068672 | tf_op jit(solution)/shard_map/all_to_all | solution.py:10
  1075.9 2.3 copy-start.12
  1077.7 1.0 copy-start.10
  1084.5 18.8 %copy-start.1 = (bf16[256,256]{1,0:T(8,128)(2,1)S(1)}, bf16[256,256]{1,0:T(8,128)(2,1)}, u32[]{:S(2)}) copy-start(bf16[256,256]{1,0:T(8,128)(2,1)} %param.13) | copy-start | bytes 393220
  1103.5 18.9 %copy-start.8 = (f32[2048]{0:T(1024)S(1)}, f32[2048]{0:T(1024)}, u32[]{:S(2)}) copy-start(f32[2048]{0:T(1024)} %param.15) | copy-start | bytes 24580
